TPU v7x, 256 devices: a whole 4x4x8 slice. The times are simulated.
256 devices in a mesh: ep: 64 (over z, y, core), tp: 4 (over x).
Axes of the slice: x: 4, y: 4, z: 8, core: 2. Of those that a mesh axis runs over, the one named last changes fastest.
Arguments:
- c_gate: bfloat16 [16384, 1024], P('ep', 'tp'), may hold values from -6 to 6
- b_gate: bfloat16 [16384, 1024], P('ep', 'tp'), may hold values from -6 to 6
- values: bfloat16 [16384, 1024], P('ep', 'tp'), may hold values from -6 to 6
- conv_taps: float32 [3, 1024], P(None, 'tp'), may hold values from -3.5 to 3.5
- w_mix_out: bfloat16 [1024, 2048], P('tp'), may hold values from -0.1875 to 0.1875
- moe_in: bfloat16 [32768, 2048], P(('ep', 'tp')), may hold values from -6 to 6
- norm_gain: float32 [2048], replicated, may hold values from 0.1 to 1.9
- route_ids: int32 [32768, 2], P(('ep', 'tp')), may hold values from 0 to 63, all different within a row; in each aligned block of 128 rows (0 to 127, 128 to 255, ...) at most 5 rows name the same one
- route_weights: float32 [32768, 2], P(('ep', 'tp')), may hold values from 0.1 to 1
- w_gate: bfloat16 [64, 2048, 3584], P('ep', None, 'tp'), may hold values from -0.125 to 0.125
- w_up: bfloat16 [64, 2048, 3584], P('ep', None, 'tp'), may hold values from -0.125 to 0.125
- w_down: bfloat16 [64, 3584, 2048], P('ep', 'tp'), may hold values from -0.09375 to 0.09375
Outputs:
- mixer_out: bfloat16 [16384, 2048], P(('ep', 'tp'))
- moe_out: bfloat16 [32768, 2048], P(('ep', 'tp'))
Inputs may be any that keep to these rules, and one draw needn't show every extreme that they name: `route_ids`: each row names 2 different experts; in each aligned block of 128 rows (the rows of one device) no expert is named by more than 5 rows, and in every draw some expert is named by exactly 5 rows in some block.
All inputs are finite; a program needn't handle non-finite values.
Results may differ from a plain program's by a relative error of at most 0.012.
Values may be sent and summed in bfloat16 or wider, within the bound.
No kernel may reach another device: no remote copies, remote signals or barrier semaphores. Data moves between devices by JAX's collectives and lax.ppermute only.
A program may use at most 128 MiB of HBM per device.

v0:
```python
import jax
import jax.numpy as jnp
from jax import lax
from jax.sharding import PartitionSpec as P

EPS = 1e-06


def passed_along(block, axis, distance):
    devices = range(lax.axis_size(axis))
    route = [(i - distance, i) for i in devices if i - distance in devices]
    return lax.ppermute(block, axis, route)


def split_up(shard, dim, length):
    before, after = (shard.shape[:dim], shard.shape[dim + 1 :])
    return jnp.moveaxis(shard.reshape(*before, length, -1, *after), dim, 0)


def sent_and_summed(shard, axis, dim):
    blocks = split_up(shard, dim, lax.axis_size(axis))
    arrived = lax.all_to_all(blocks, axis, split_axis=0, concat_axis=0, tiled=True)
    return arrived.astype(jnp.float32).sum(axis=0)


def rank_copies(route_block, experts):
    flat_ids = route_block.reshape(-1)
    onehot = (flat_ids[:, None] == jnp.arange(experts, dtype=jnp.int32)[None, :]).astype(jnp.int32)
    before = jnp.cumsum(onehot, axis=0) - onehot
    return (flat_ids, jnp.sum(before * onehot, axis=1))


def pack_rows(rows, slot_of, top, slot_count):
    copies = slot_of.shape[0]
    table = (
        jnp.full((slot_count,), copies, jnp.int32)
        .at[slot_of]
        .set(jnp.arange(copies, dtype=jnp.int32))
    )
    padded = jnp.concatenate([rows, jnp.zeros((1, rows.shape[1]), rows.dtype)], 0)
    return padded[table // top]


def on_device(
    c_gate,
    b_gate,
    values,
    conv_taps,
    w_mix_out,
    moe_in,
    norm_gain,
    route_ids,
    route_weights,
    w_gate,
    w_up,
    w_down,
):
    tokens = c_gate.shape[0]
    reach = conv_taps.shape[0] - 1
    product = c_gate.astype(jnp.float32) * values.astype(jnp.float32)
    previous = passed_along(product[tokens - reach :], "ep", 1)
    extended = jnp.concatenate([previous, product], 0)
    convolved = jnp.zeros_like(product)
    for offset in range(reach + 1):
        convolved = convolved + conv_taps[offset][None, :] * extended[offset : offset + tokens]
    mixed = (b_gate.astype(jnp.float32) * convolved).astype(jnp.bfloat16)
    piece = mixed
    mixer_out = sent_and_summed(
        jnp.dot(piece, w_mix_out, preferred_element_type=jnp.float32).astype(jnp.bfloat16), "tp", 0
    ).astype(jnp.bfloat16)
    rows_b = moe_in.shape[0]
    width = moe_in.shape[1]
    top = route_ids.shape[1]
    n_ep = lax.axis_size("ep")
    experts = w_gate.shape[0] * n_ep
    capacity = 5 * rows_b * top // (4 * experts)
    stream = moe_in.astype(jnp.float32)
    scale = lax.rsqrt(jnp.mean(stream * stream, axis=1, keepdims=True) + EPS)
    normed = (stream * scale * norm_gain[None, :]).astype(jnp.bfloat16)
    own_ids, own_ranks = rank_copies(route_ids, experts)
    own_slot = own_ids * capacity + own_ranks
    outgoing = pack_rows(normed, own_slot, top, experts * capacity).reshape(
        experts, capacity, width
    )
    arrived = lax.all_to_all(outgoing, "ep", split_axis=0, concat_axis=1, tiled=True).reshape(
        -1, width
    )
    piece = lax.all_gather(arrived, "tp", axis=0, tiled=True)
    gate_val = jnp.dot(piece, w_gate[0], preferred_element_type=jnp.float32)
    up_val = jnp.dot(piece, w_up[0], preferred_element_type=jnp.float32)
    hidden = (jax.nn.silu(gate_val) * up_val).astype(jnp.bfloat16)
    piece = hidden
    expert_out = sent_and_summed(
        jnp.dot(piece, w_down[0], preferred_element_type=jnp.float32).astype(jnp.bfloat16), "tp", 0
    ).astype(jnp.bfloat16)
    returned = lax.all_to_all(
        expert_out.reshape(n_ep, capacity, width), "ep", split_axis=0, concat_axis=0, tiled=True
    )
    picked = returned.reshape(-1, width)[own_slot].astype(jnp.float32).reshape(rows_b, top, width)
    moe_out = jnp.sum(picked * route_weights[:, :, None], axis=1).astype(jnp.bfloat16)
    return (mixer_out, moe_out)


def solution(mesh):
    return jax.shard_map(
        on_device,
        mesh=mesh,
        in_specs=(
            P("ep", "tp"),
            P("ep", "tp"),
            P("ep", "tp"),
            P(None, "tp"),
            P("tp", None),
            P(("ep", "tp"), None),
            P(),
            P(("ep", "tp"), None),
            P(("ep", "tp"), None),
            P("ep", None, "tp"),
            P("ep", None, "tp"),
            P("ep", "tp", None),
        ),
        out_specs=(P(("ep", "tp"), None), P(("ep", "tp"), None)),
        check_vma=False,
    )
```

profile of v0, /device:TPU:8, one launch (start us, length us, event | category | flops | bytes accessed | tf_op | source)
XLA Modules:
  0.0 333.2 jit_solution(17508996634302096302)
XLA Ops:
  7.2 0.0 copy-start
  7.2 0.0 all-gather.2.cloned.1.call-start
  7.2 0.9 copy.16
  8.1 0.1 eq.29
  8.2 0.1 eq.25
  8.4 0.7 broadcast_multiply_fusion
  9.1 0.6 reduce-window.6
  9.7 0.2 slice_reduce_fusion
  9.9 0.1 copy.15
  10.0 0.1 mul.107
  10.2 0.1 fusion.20
  10.3 1.4 scatter_custom_fusion
  11.7 1.2 fusion.4
  13.0 1.2 fusion.6
  14.3 3.0 gather_fusion
  17.3 2.4 reshape.88
  19.7 63.2 %all_to_all.24 = bf16[64,5,2048]{2,1,0:T(8,128)(2,1)} all-to-all(bf16[64,5,2048]{2,1,0:T(8,128)(2,1)S(1)} %reshape.88), channel_id=1, replica_groups=mesh['ep'=64,'tp'=4] {'ep'}, dimensions={0} | all-to-all | bytes 2621440 | tf_op jit(solution)/shard_map/all_to_all | solution.py:85
  82.9 3.7 %reshape.89 = bf16[320,2048]{1,0:T(8,128)(2,1)} reshape(bf16[64,5,2048]{2,1,0:T(8,128)(2,1)} %all_to_all.24) | data formatting | bytes 2621440 | tf_op jit(solution)/shard_map/reshape | solution.py:85
  86.6 0.0 all-gather.2.cloned.1.call-update
  86.6 55.8 %all-gather.2.cloned.1.call-done = bf16[1280,2048]{1,0:T(8,128)(2,1)} async-done(((bf16[320,2048]{1,0:T(8,128)(2,1)}), bf16[1280,2048]{1,0:T(8,128)(2,1)}) %all-gather.2.cloned.1.call-update) | async-done | bytes 5242896 | tf_op jit(solution)/shard_map/all_gather | solution.py:88
  142.4 10.0 %fusion.2 = f32[1280,896]{1,0:T(8,128)} fusion(bf16[1280,2048]{1,0:T(8,128)(2,1)} %all-gather.2.cloned.1.call-done, bf16[1,2048,896]{2,1,0:T(8,128)(2,1)} %param.21), kind=kOutput, calls=%fused_computation.7 | convolution fusion | flops 4697620480 | bytes 13500416 | tf_op jit(solution)/shard_map/dot_general | solution.py:89
  152.4 17.5 %convolution_convert_fusion = bf16[1280,2048]{1,0:T(8,128)(2,1)} fusion(bf16[1,896,2048]{2,1,0:T(8,128)(2,1)} %param.23, f32[1280,896]{1,0:T(8,128)} %fusion.2, bf16[1280,2048]{1,0:T(8,128)(2,1)} %all-gather.2.cloned.1.call-done, bf16[1,2048,896]{2,1,0:T(8,128)(2,1)} %param.22), kind=kOutput, calls=%fused_computation.3 | convolution fusion | flops 9404743680 | bytes 22413312 | tf_op jit(solution)/shard_map/dot_general | solution.py:94
  169.9 0.0 copy-start.2
  169.9 0.0 copy-start.3
  169.9 0.0 copy-start.4
  169.9 0.0 copy-start.1
  169.9 5.2 %all-to-all-start.2 = ((bf16[4,320,2048]{2,1,0:T(8,128)(2,1)}), bf16[4,320,2048]{2,1,0:T(8,128)(2,1)}, u32[]{:S(2)}, u32[]{:S(2)}) async-start(bf16[4,320,2048]{2,1,0:T(8,128)(2,1)} %bitcast.47), calls=%async_computation.2 | async-start | bytes 10485760 | tf_op jit(solution)/shard_map/all_to_all | solution.py:22
  175.1 0.0 copy-done.2
  175.2 0.0 copy-done.3
  175.2 1.9 collective-permute-start
  177.1 0.0 copy-done.4
  177.2 3.0 collective-permute-done
  180.1 0.0 copy-done
  180.1 0.0 copy-done.1
  180.1 1.5 convolution_convert_fusion.1
  181.6 53.8 %all-to-all-done.2 = bf16[4,320,2048]{2,1,0:T(8,128)(2,1)} async-done(((bf16[4,320,2048]{2,1,0:T(8,128)(2,1)}), bf16[4,320,2048]{2,1,0:T(8,128)(2,1)}, u32[]{:S(2)}, u32[]{:S(2)}) %all-to-all-start.2) | async-done | bytes 5242912 | tf_op jit(solution)/shard_map/all_to_all | solution.py:22
  235.4 3.7 %all-to-all-start = ((bf16[4,64,2048]{2,1,0:T(8,128)(2,1)}), bf16[4,64,2048]{2,1,0:T(8,128)(2,1)S(1)}, u32[]{:S(2)}, u32[]{:S(2)}) async-start(bf16[4,64,2048]{2,1,0:T(8,128)(2,1)} %bitcast.3), calls=%async_computation | async-start | bytes 2097152 | tf_op jit(solution)/shard_map/all_to_all | solution.py:22
  239.1 3.6 %reduce_sum.57 = bf16[320,2048]{1,0:T(8,128)(2,1)S(1)} reduce(bf16[4,320,2048]{2,1,0:T(8,128)(2,1)} %all-to-all-done.2, bf16[]{:T(256)} %constant.18.clone.1), dimensions={0}, to_apply=%region_6.7 | reduce | flops 1966080 | bytes 6553602 | tf_op jit(solution)/shard_map/reduce_sum | solution.py:23
  242.7 0.0 copy-start.5
  242.7 1.6 reshape.91
  244.3 8.9 %all-to-all-done = bf16[4,64,2048]{2,1,0:T(8,128)(2,1)S(1)} async-done(((bf16[4,64,2048]{2,1,0:T(8,128)(2,1)}), bf16[4,64,2048]{2,1,0:T(8,128)(2,1)S(1)}, u32[]{:S(2)}, u32[]{:S(2)}) %all-to-all-start) | async-done | bytes 1048608 | tf_op jit(solution)/shard_map/all_to_all | solution.py:22
  253.2 10.7 %all-to-all-start.3 = ((bf16[64,5,2048]{2,1,0:T(8,128)(2,1)}), bf16[64,5,2048]{2,1,0:T(8,128)(2,1)}, u32[]{:S(2)}, u32[]{:S(2)}) async-start(bf16[64,5,2048]{2,1,0:T(8,128)(2,1)} %reshape.91), calls=%async_computation.3 | async-start | bytes 4194304 | tf_op jit(solution)/shard_map/all_to_all | solution.py:96
  263.9 0.0 copy-done.5
  264.0 0.1 copy.19
  264.1 0.9 reduce_sum.53
  265.0 50.1 %all-to-all-done.3 = bf16[64,5,2048]{2,1,0:T(8,128)(2,1)} async-done(((bf16[64,5,2048]{2,1,0:T(8,128)(2,1)}), bf16[64,5,2048]{2,1,0:T(8,128)(2,1)}, u32[]{:S(2)}, u32[]{:S(2)}) %all-to-all-start.3) | async-done | bytes 1310752 | tf_op jit(solution)/shard_map/all_to_all | solution.py:96
  315.1 2.6 reshape.92
  317.7 2.3 gather_fusion.1
  320.0 2.4 reshape.93
  322.4 3.9 %multiply_reduce_fusion = bf16[128,2048]{1,0:T(8,128)(2,1)} fusion(f32[128,2,2048]{2,1,0:T(2,128)S(1)} %reshape.93, f32[128,2]{1,0:T(8,128)S(1)} %copy.19), kind=kLoop, calls=%fused_computation.10 | loop fusion | flops 786432 | bytes 2622464 | tf_op jit(solution)/shard_map/reduce_sum | solution.py:100
  (13 shorter events, 0.2 us)
Async XLA Ops:
  7.2 173.0 %copy-start = (bf16[256,2048]{1,0:T(8,128)(2,1)S(1)}, bf16[256,2048]{1,0:T(8,128)(2,1)}, u32[]{:S(2)}) copy-start(bf16[256,2048]{1,0:T(8,128)(2,1)} %param.16) | copy-start | bytes 3145732
  7.2 135.2 %all-gather.2.cloned.1.call-start = ((), (), s32[]{:S(2)}) async-start(), calls=%async_computation.4 | async-start | bytes 6553600 | tf_op jit(solution)/shard_map/all_gather | solution.py:88
  169.9 5.3 %copy-start.2 = (bf16[256,256]{1,0:T(8,128)(2,1)S(1)}, bf16[256,256]{1,0:T(8,128)(2,1)}, u32[]{:S(2)}) copy-start(bf16[256,256]{1,0:T(8,128)(2,1)} %param.14) | copy-start | bytes 393220
  169.9 5.3 %copy-start.3 = (bf16[256,256]{1,0:T(8,128)(2,1)S(1)}, bf16[256,256]{1,0:T(8,128)(2,1)}, u32[]{:S(2)}) copy-start(bf16[256,256]{1,0:T(8,128)(2,1)} %param.12) | copy-start | bytes 393220
  169.9 7.2 %copy-start.4 = (f32[3,256]{1,0:T(4,128)S(1)}, f32[3,256]{1,0:T(4,128)}, u32[]{:S(2)}) copy-start(f32[3,256]{1,0:T(4,128)} %param.15) | copy-start | bytes 9220
  169.9 10.2 %copy-start.1 = (bf16[256,256]{1,0:T(8,128)(2,1)S(1)}, bf16[256,256]{1,0:T(8,128)(2,1)}, u32[]{:S(2)}) copy-start(bf16[256,256]{1,0:T(8,128)(2,1)} %param.13) | copy-start | bytes 393220
  169.9 65.4 %all-to-all-start.2 = ((bf16[4,320,2048]{2,1,0:T(8,128)(2,1)}), bf16[4,320,2048]{2,1,0:T(8,128)(2,1)}, u32[]{:S(2)}, u32[]{:S(2)}) async-start(bf16[4,320,2048]{2,1,0:T(8,128)(2,1)} %bitcast.47), calls=%async_computation.2 | async-start | bytes 10485760 | tf_op jit(solution)/shard_map/all_to_all | solution.py:22
  175.2 4.9 %collective-permute-start = (f32[2,256]{1,0:T(2,128)S(1)}, f32[2,256]{1,0:T(2,128)S(1)}, u32[]{:S(2)}, u32[]{:S(2)}) collective-permute-start(f32[2,256]{1,0:T(2,128)S(1)} %slice.36), channel_id=1, source_target_pairs={{0,4},{4,8},{8,12},{12,16},{16,20},{20,24},{24,28},{28,32},{32,36}... | collective-permute-start | bytes 6152 | tf_op jit(solution)/shard_map/ppermute | solution.py:12
  235.4 17.8 %all-to-all-start = ((bf16[4,64,2048]{2,1,0:T(8,128)(2,1)}), bf16[4,64,2048]{2,1,0:T(8,128)(2,1)S(1)}, u32[]{:S(2)}, u32[]{:S(2)}) async-start(bf16[4,64,2048]{2,1,0:T(8,128)(2,1)} %bitcast.3), calls=%async_computation | async-start | bytes 2097152 | tf_op jit(solution)/shard_map/all_to_all | solution.py:22
  242.7 21.3 %copy-start.5 = (f32[128,2]{0,1:T(2,128)S(1)}, f32[128,2]{0,1:T(2,128)}, u32[]{:S(2)}) copy-start(f32[128,2]{0,1:T(2,128)} %param.20) | copy-start | bytes 3076
  253.2 61.9 %all-to-all-start.3 = ((bf16[64,5,2048]{2,1,0:T(8,128)(2,1)}), bf16[64,5,2048]{2,1,0:T(8,128)(2,1)}, u32[]{:S(2)}, u32[]{:S(2)}) async-start(bf16[64,5,2048]{2,1,0:T(8,128)(2,1)} %reshape.91), calls=%async_computation.3 | async-start | bytes 4194304 | tf_op jit(solution)/shard_map/all_to_all | solution.py:96
Sparse Core Ops, SparseCore 0:
  86.7 55.6 all-gather.1
where the time goes:
time: 334 us; the launch traced here: 333 us
  waiting for transfers between devices  172 us (51%)
  blocking collectives  63.2 us (19%)
  matrix products  29 us (9%)
  starting transfers between devices  21.6 us (6%)
  local copies, waits for them, and re-layouts  21.1 us (6%)
  between operations  14.2 us (4%)
  other arithmetic  12.4 us (4%)
    all_to_all x1, blocking collectives, on_device(): lax.all_to_all(outgoing, 'ep', split_axis=0, concat_axis=1, tiled=True)  63.2 us
    all_to_all x2, waiting for transfers between devices, sent_and_summed(): lax.all_to_all(blocks, axis, split_axis=0, concat_axis=0, tiled=True)  62.6 us
    all_gather x1, waiting for transfers between devices, on_device(): piece = lax.all_gather(arrived, 'tp', axis=0, tiled=True)  55.8 us
    all_to_all x1, waiting for transfers between devices, on_device(): lax.all_to_all(expert_out.reshape(n_ep, capacity, width), 'ep', split_axi...  50.1 us
    dot_general x1, matrix products, on_device(): jnp.dot(piece, w_down[0], preferred_element_type=jnp.float32)  17.5 us
    all_to_all x1, starting transfers between devices, on_device(): lax.all_to_all(expert_out.reshape(n_ep, capacity, width), 'ep', split_axi...  10.7 us
    dot_general x1, matrix products, on_device(): gate_val = jnp.dot(piece, w_gate[0], preferred_element_type=jnp.float32)  9.98 us
    all_to_all x2, starting transfers between devices, sent_and_summed(): lax.all_to_all(blocks, axis, split_axis=0, concat_axis=0, tiled=True)  8.91 us
  transfers between devices with their start and end apart: 5, of which 5 were waited for; matrix products, arithmetic and copies ran while one was open for 2% of the time, Pallas kernels for 0%

commit v1 on v0

--- a/solution.py
+++ b/solution.py
@@ -85,7 +85,9 @@
     arrived = lax.all_to_all(outgoing, "ep", split_axis=0, concat_axis=1, tiled=True).reshape(
         -1, width
     )
-    piece = lax.all_gather(arrived, "tp", axis=0, tiled=True)
+    piece = jnp.concatenate(
+        lax.all_to_all(jnp.stack([arrived] * lax.axis_size("tp")), "tp", 0, 0), axis=0
+    )
     gate_val = jnp.dot(piece, w_gate[0], preferred_element_type=jnp.float32)
     up_val = jnp.dot(piece, w_up[0], preferred_element_type=jnp.float32)
     hidden = (jax.nn.silu(gate_val) * up_val).astype(jnp.bfloat16)

time: 334 us -> 323 us (0.967)
  blocking collectives: 63.2 us -> 126 us
  waiting for transfers between devices: 172 us -> 111 us
  between operations: 14.2 us -> 0.88 us
    all_to_all x0 -> x1, blocking collectives: none -> 62.9 us  [on_device(): lax.all_to_all(jnp.stack([arrived] * lax.axis_size('tp')), 'tp', 0, 0)]
    all_gather x1 -> x0, waiting for transfers between devices: 55.8 us -> none  [on_device(): piece = lax.all_gather(arrived, 'tp', axis=0, tiled=True)]
    all_to_all x2, waiting for transfers between devices: 62.6 us -> 57.7 us  [sent_and_summed(): lax.all_to_all(blocks, axis, split_axis=0, concat_axis=0, tiled=True)]
    reshape x1 -> x0, local copies, waits for them, and re-layouts: 3.66 us -> none  [on_device(): lax.all_to_all(outgoing, 'ep', split_axis=0, concat_axis=1, tiled=True)]
  transfers between devices with their start and end apart: 5 -> 4, of which waited for: 5 -> 4; matrix products, arithmetic and copies ran while one was open for 2% -> 2% of each run, Pallas kernels for 0% -> 0%
where the time goes in v1:
time: 323 us; the launch traced here: 322 us
  blocking collectives  126 us (39%)
  waiting for transfers between devices  111 us (34%)
  matrix products  26.1 us (8%)
  starting transfers between devices  23.1 us (7%)
  local copies, waits for them, and re-layouts  23 us (7%)
  other arithmetic  12.4 us (4%)
    all_to_all x1, blocking collectives, on_device(): lax.all_to_all(outgoing, 'ep', split_axis=0, concat_axis=1, tiled=True)  63.2 us
    all_to_all x1, blocking collectives, on_device(): lax.all_to_all(jnp.stack([arrived] * lax.axis_size('tp')), 'tp', 0, 0)  62.9 us
    all_to_all x2, waiting for transfers between devices, sent_and_summed(): lax.all_to_all(blocks, axis, split_axis=0, concat_axis=0, tiled=True)  57.7 us
    all_to_all x1, waiting for transfers between devices, on_device(): lax.all_to_all(expert_out.reshape(n_ep, capacity, width), 'ep', split_axi...  50.1 us
    dot_general x1, matrix products, on_device(): jnp.dot(piece, w_down[0], preferred_element_type=jnp.float32)  17.5 us
    all_to_all x1, starting transfers between devices, on_device(): lax.all_to_all(expert_out.reshape(n_ep, capacity, width), 'ep', split_axi...  12.3 us
    all_to_all x2, starting transfers between devices, sent_and_summed(): lax.all_to_all(blocks, axis, split_axis=0, concat_axis=0, tiled=True)  8.91 us
    dot_general x1, matrix products, on_device(): gate_val = jnp.dot(piece, w_gate[0], preferred_element_type=jnp.float32)  7.14 us
  transfers between devices with their start and end apart: 4, of which 4 were waited for; matrix products, arithmetic and copies ran while one was open for 2% of the time, Pallas kernels for 0%

profile of v1, /device:TPU:8, one launch (start us, length us, event | category | flops | bytes accessed | tf_op | source)
XLA Modules:
  0.0 322.5 jit_solution(671714827138857520)
XLA Ops:
  0.6 0.0 copy-start
  0.6 0.9 copy.16
  1.5 0.1 eq.29
  1.7 0.1 eq.25
  1.8 0.7 broadcast_multiply_fusion
  2.5 0.6 reduce-window.6
  3.1 0.2 slice_reduce_fusion
  3.3 0.1 copy.15
  3.5 0.1 mul.107
  3.6 0.1 fusion.20
  3.7 1.4 scatter_custom_fusion
  5.2 1.2 fusion.4
  6.4 1.2 fusion.6
  7.7 3.0 gather_fusion
  10.7 2.4 reshape.89
  13.1 63.2 %all_to_all.32 = bf16[64,5,2048]{2,1,0:T(8,128)(2,1)} all-to-all(bf16[64,5,2048]{2,1,0:T(8,128)(2,1)S(1)} %reshape.89), channel_id=1, replica_groups=mesh['ep'=64,'tp'=4] {'ep'}, dimensions={0} | all-to-all | bytes 2621440 | tf_op jit(solution)/shard_map/all_to_all | solution.py:85
  76.3 2.6 all_to_all.23
  78.9 0.6 stack.3
  79.6 0.0 copy-start.7
  79.6 62.9 %all_to_all.33 = bf16[4,320,2048]{2,1,0:T(8,128)(2,1)S(1)} all-to-all(bf16[4,320,2048]{2,1,0:T(8,128)(2,1)S(1)} %stack.3), channel_id=1, replica_groups=mesh['ep'=64,'tp'=4] {'tp'}, dimensions={0} | all-to-all | bytes 10485760 | tf_op jit(solution)/shard_map/all_to_all | solution.py:89
  142.4 0.0 copy-start.1
  142.4 2.3 copy-done.1
  144.8 0.0 copy-done.7
  144.8 7.1 %fusion.2 = f32[1280,896]{1,0:T(8,128)} fusion(bf16[1280,2048]{1,0:T(8,128)(2,1)S(1)} %bitcast.49, bf16[1,2048,896]{2,1,0:T(8,128)(2,1)S(1)} %copy-done.7), kind=kOutput, calls=%fused_computation.7 | convolution fusion | flops 4697620480 | bytes 13500416 | tf_op jit(solution)/shard_map/dot_general | solution.py:91
  151.9 17.5 %convolution_convert_fusion = bf16[1280,2048]{1,0:T(8,128)(2,1)} fusion(bf16[1,896,2048]{2,1,0:T(8,128)(2,1)} %param.23, f32[1280,896]{1,0:T(8,128)} %fusion.2, bf16[1280,2048]{1,0:T(8,128)(2,1)} %bitcast.50, bf16[1,2048,896]{2,1,0:T(8,128)(2,1)} %param.22), kind=kOutput, calls=%fused_computation.3 | convolution fusion | flops 9404743680 | bytes 22413312 | tf_op jit(solution)/shard_map/dot_general | solution.py:96
  169.5 0.0 copy-start.3
  169.5 0.0 copy-start.4
  169.5 0.0 copy-start.5
  169.5 0.0 copy-start.2
  169.5 5.2 %all-to-all-start.3 = ((bf16[4,320,2048]{2,1,0:T(8,128)(2,1)}), bf16[4,320,2048]{2,1,0:T(8,128)(2,1)}, u32[]{:S(2)}, u32[]{:S(2)}) async-start(bf16[4,320,2048]{2,1,0:T(8,128)(2,1)} %bitcast.48), calls=%async_computation.3 | async-start | bytes 10485760 | tf_op jit(solution)/shard_map/all_to_all | solution.py:22
  174.7 0.0 copy-done.3
  174.7 0.0 copy-done.4
  174.8 1.9 collective-permute-start
  176.7 0.0 copy-done.5
  176.7 3.0 collective-permute-done
  179.7 0.0 copy-done
  179.7 0.0 copy-done.2
  179.7 1.5 convolution_convert_fusion.1
  181.1 51.3 %all-to-all-done.3 = bf16[4,320,2048]{2,1,0:T(8,128)(2,1)} async-done(((bf16[4,320,2048]{2,1,0:T(8,128)(2,1)}), bf16[4,320,2048]{2,1,0:T(8,128)(2,1)}, u32[]{:S(2)}, u32[]{:S(2)}) %all-to-all-start.3) | async-done | bytes 5242912 | tf_op jit(solution)/shard_map/all_to_all | solution.py:22
  232.4 3.7 %all-to-all-start = ((bf16[4,64,2048]{2,1,0:T(8,128)(2,1)}), bf16[4,64,2048]{2,1,0:T(8,128)(2,1)S(1)}, u32[]{:S(2)}, u32[]{:S(2)}) async-start(bf16[4,64,2048]{2,1,0:T(8,128)(2,1)} %bitcast.3), calls=%async_computation | async-start | bytes 2097152 | tf_op jit(solution)/shard_map/all_to_all | solution.py:22
  236.1 3.6 %reduce_sum.57 = bf16[320,2048]{1,0:T(8,128)(2,1)S(1)} reduce(bf16[4,320,2048]{2,1,0:T(8,128)(2,1)} %all-to-all-done.3, bf16[]{:T(256)} %constant.18.clone.1), dimensions={0}, to_apply=%region_6.7 | reduce | flops 1966080 | bytes 6553602 | tf_op jit(solution)/shard_map/reduce_sum | solution.py:23
  239.8 0.0 copy-start.6
  239.8 1.6 reshape.92
  241.4 6.4 %all-to-all-done = bf16[4,64,2048]{2,1,0:T(8,128)(2,1)S(1)} async-done(((bf16[4,64,2048]{2,1,0:T(8,128)(2,1)}), bf16[4,64,2048]{2,1,0:T(8,128)(2,1)S(1)}, u32[]{:S(2)}, u32[]{:S(2)}) %all-to-all-start) | async-done | bytes 1048608 | tf_op jit(solution)/shard_map/all_to_all | solution.py:22
  247.8 12.3 %all-to-all-start.4 = ((bf16[64,5,2048]{2,1,0:T(8,128)(2,1)}), bf16[64,5,2048]{2,1,0:T(8,128)(2,1)}, u32[]{:S(2)}, u32[]{:S(2)}) async-start(bf16[64,5,2048]{2,1,0:T(8,128)(2,1)} %reshape.92), calls=%async_computation.4 | async-start | bytes 4194304 | tf_op jit(solution)/shard_map/all_to_all | solution.py:98
  260.1 0.0 copy-done.6
  260.1 0.1 copy.19
  260.2 0.9 reduce_sum.53
  261.2 50.1 %all-to-all-done.4 = bf16[64,5,2048]{2,1,0:T(8,128)(2,1)} async-done(((bf16[64,5,2048]{2,1,0:T(8,128)(2,1)}), bf16[64,5,2048]{2,1,0:T(8,128)(2,1)}, u32[]{:S(2)}, u32[]{:S(2)}) %all-to-all-start.4) | async-done | bytes 1310752 | tf_op jit(solution)/shard_map/all_to_all | solution.py:98
  311.3 2.6 reshape.93
  313.8 2.3 gather_fusion.1
  316.2 2.4 reshape.94
  318.5 3.9 %multiply_reduce_fusion = bf16[128,2048]{1,0:T(8,128)(2,1)} fusion(f32[128,2,2048]{2,1,0:T(2,128)S(1)} %reshape.94, f32[128,2]{1,0:T(8,128)S(1)} %copy.19), kind=kLoop, calls=%fused_computation.10 | loop fusion | flops 786432 | bytes 2622464 | tf_op jit(solution)/shard_map/reduce_sum | solution.py:102
  (13 shorter events, 0.2 us)
Async XLA Ops:
  0.6 179.1 %copy-start = (bf16[256,2048]{1,0:T(8,128)(2,1)S(1)}, bf16[256,2048]{1,0:T(8,128)(2,1)}, u32[]{:S(2)}) copy-start(bf16[256,2048]{1,0:T(8,128)(2,1)} %param.16) | copy-start | bytes 3145732
  79.6 65.2 %copy-start.7 = (bf16[1,2048,896]{2,1,0:T(8,128)(2,1)S(1)}, bf16[1,2048,896]{2,1,0:T(8,128)(2,1)}, u32[]{:S(2)}) copy-start(bf16[1,2048,896]{2,1,0:T(8,128)(2,1)} %param.21) | copy-start | bytes 11010052
  142.4 2.3 copy-start.1
  169.5 5.3 %copy-start.3 = (bf16[256,256]{1,0:T(8,128)(2,1)S(1)}, bf16[256,256]{1,0:T(8,128)(2,1)}, u32[]{:S(2)}) copy-start(bf16[256,256]{1,0:T(8,128)(2,1)} %param.14) | copy-start | bytes 393220
  169.5 5.3 %copy-start.4 = (bf16[256,256]{1,0:T(8,128)(2,1)S(1)}, bf16[256,256]{1,0:T(8,128)(2,1)}, u32[]{:S(2)}) copy-start(bf16[256,256]{1,0:T(8,128)(2,1)} %param.12) | copy-start | bytes 393220
  169.5 7.2 %copy-start.5 = (f32[3,256]{1,0:T(4,128)S(1)}, f32[3,256]{1,0:T(4,128)}, u32[]{:S(2)}) copy-start(f32[3,256]{1,0:T(4,128)} %param.15) | copy-start | bytes 9220
  169.5 10.2 %copy-start.2 = (bf16[256,256]{1,0:T(8,128)(2,1)S(1)}, bf16[256,256]{1,0:T(8,128)(2,1)}, u32[]{:S(2)}) copy-start(bf16[256,256]{1,0:T(8,128)(2,1)} %param.13) | copy-start | bytes 393220
  169.5 62.9 %all-to-all-start.3 = ((bf16[4,320,2048]{2,1,0:T(8,128)(2,1)}), bf16[4,320,2048]{2,1,0:T(8,128)(2,1)}, u32[]{:S(2)}, u32[]{:S(2)}) async-start(bf16[4,320,2048]{2,1,0:T(8,128)(2,1)} %bitcast.48), calls=%async_computation.3 | async-start | bytes 10485760 | tf_op jit(solution)/shard_map/all_to_all | solution.py:22
  174.8 4.9 %collective-permute-start = (f32[2,256]{1,0:T(2,128)S(1)}, f32[2,256]{1,0:T(2,128)S(1)}, u32[]{:S(2)}, u32[]{:S(2)}) collective-permute-start(f32[2,256]{1,0:T(2,128)S(1)} %slice.36), channel_id=1, source_target_pairs={{0,4},{4,8},{8,12},{12,16},{16,20},{20,24},{24,28},{28,32},{32,36}... | collective-permute-start | bytes 6152 | tf_op jit(solution)/shard_map/ppermute | solution.py:12
  232.4 15.4 %all-to-all-start = ((bf16[4,64,2048]{2,1,0:T(8,128)(2,1)}), bf16[4,64,2048]{2,1,0:T(8,128)(2,1)S(1)}, u32[]{:S(2)}, u32[]{:S(2)}) async-start(bf16[4,64,2048]{2,1,0:T(8,128)(2,1)} %bitcast.3), calls=%async_computation | async-start | bytes 2097152 | tf_op jit(solution)/shard_map/all_to_all | solution.py:22
  239.8 20.3 %copy-start.6 = (f32[128,2]{0,1:T(2,128)S(1)}, f32[128,2]{0,1:T(2,128)}, u32[]{:S(2)}) copy-start(f32[128,2]{0,1:T(2,128)} %param.20) | copy-start | bytes 3076
  247.8 63.5 %all-to-all-start.4 = ((bf16[64,5,2048]{2,1,0:T(8,128)(2,1)}), bf16[64,5,2048]{2,1,0:T(8,128)(2,1)}, u32[]{:S(2)}, u32[]{:S(2)}) async-start(bf16[64,5,2048]{2,1,0:T(8,128)(2,1)} %reshape.92), calls=%async_computation.4 | async-start | bytes 4194304 | tf_op jit(solution)/shard_map/all_to_all | solution.py:98
